TPU v7x, 32 devices: a whole 2x2x4 slice. The times are simulated.
32 devices in a mesh: rep: 2 (over x), fs: 4 (over z), tp: 4 (over y, core).
Axes of the slice: x: 2, y: 2, z: 4, core: 2. Of those that a mesh axis runs over, the one named last changes fastest.
Arguments:
- residual: bfloat16 [8, 768, 4, 512], P(('rep', 'fs'), None, None, 'tp'), may hold values from -6 to 6
- mixer_gain: float32 [4, 512], P(None, 'tp'), may hold values from 0.1 to 1.9
- pool_weight: float32 [4, 512, 512], P(None, 'fs', 'tp'), may hold values from -0.25 to 0.25
- pool_scale: float32 [4, 512], P(None, 'tp'), may hold values from 0.5 to 2
- channel_gain: float32 [4, 512], P(None, 'tp'), may hold values from 0.1 to 1.9
- gate_weight: float32 [2048, 6144], P('fs', 'tp'), may hold values from -0.125 to 0.125
- up_weight: float32 [2048, 6144], P('fs', 'tp'), may hold values from -0.125 to 0.125
- gate_scale: float32 [4, 1536], P('fs', 'tp'), may hold values from 0.5 to 2
- up_scale: float32 [4, 1536], P('fs', 'tp'), may hold values from 0.5 to 2
- gate_taps: float32 [3, 6144], P(None, 'tp'), may hold values from -3.5 to 3.5
- up_taps: float32 [3, 6144], P(None, 'tp'), may hold values from -3.5 to 3.5
- down_weight: float32 [6144, 2048], P('tp', 'fs'), may hold values from -0.078125 to 0.078125
- down_scale: float32 [4, 512], P(None, 'tp'), may hold values from 0.5 to 2
Outputs:
- layer_out: bfloat16 [8, 768, 4, 512], P(('rep', 'fs'), None, None, 'tp')
All inputs are finite; a program needn't handle non-finite values.
Results may differ from a plain program's by a relative error of at most 0.018.
Values may be sent and summed in bfloat16 or wider, within the bound.
A program may use at most 128 MiB of HBM per device.

v0:
```python
import jax
import jax.numpy as jnp
from jax import lax
from jax.sharding import PartitionSpec as P

WINDOWS = (2, 4, 8, 16)
EPSILON = 1e-05


def shifted(values, steps):
    padding = jnp.zeros((steps,) + values.shape[1:], values.dtype)
    return jnp.concatenate([padding, values[:-steps]], axis=0)


def pooled_groups(normed):
    values = normed.astype(jnp.float32)
    totals = values
    reach_now = 1
    columns = []
    positions = jnp.arange(1, values.shape[0] + 1).astype(jnp.float32)
    for group_idx in range(len(WINDOWS)):
        while reach_now < WINDOWS[group_idx]:
            totals = totals + shifted(totals, reach_now)
            reach_now = reach_now * 2
        divisor = jnp.minimum(positions, float(WINDOWS[group_idx]))
        columns.append(totals[:, group_idx] / divisor[:, None] - values[:, group_idx])
    return jnp.stack(columns, axis=1).astype(jnp.bfloat16)


def local_square(values):
    return jnp.sum(values * values, axis=(1, 2), keepdims=True)


def scaled(values, total, width_all, gain):
    return (values * lax.rsqrt(total / width_all + EPSILON) * gain).astype(jnp.bfloat16)


def causal_taps(stored, taps):
    values = stored.astype(jnp.float32)
    return taps[2] * values + taps[1] * shifted(values, 1) + taps[0] * shifted(values, 2)


def shards(
    residual,
    mixer_gain,
    pool_weight,
    pool_scale,
    channel_gain,
    gate_weight,
    up_weight,
    gate_scale,
    up_scale,
    gate_taps,
    up_taps,
    down_weight,
    down_scale,
):
    sequence = residual[0]
    length = sequence.shape[0]
    groups = sequence.shape[1]
    local_width = sequence.shape[2]
    width_all = groups * local_width * lax.axis_size("tp")
    pool_rows = lax.all_gather(pool_weight.astype(jnp.bfloat16), "fs", axis=1, tiled=True)
    values = sequence.astype(jnp.float32)
    total = lax.psum(local_square(values), "tp")
    pooled = pooled_groups(scaled(values, total, width_all, mixer_gain))
    mixed = jnp.einsum(
        "lgc,gce->lge",
        lax.all_gather(pooled, "tp", axis=2, tiled=True),
        pool_rows,
        preferred_element_type=jnp.float32,
    )
    middle = (mixed * pool_scale + values).astype(jnp.bfloat16)
    middle_values = middle.astype(jnp.float32)
    middle_total = lax.psum(local_square(middle_values), "tp")
    inputs_local = scaled(middle_values, middle_total, width_all, channel_gain)
    inputs = lax.all_gather(inputs_local, "tp", axis=2, tiled=True).reshape(length, -1)
    scale_pair = (
        lax.all_gather(gate_scale, "fs", axis=0, tiled=True),
        lax.all_gather(up_scale, "fs", axis=0, tiled=True),
    )
    gate_columns = scale_pair[0].reshape(-1)
    up_columns = scale_pair[1].reshape(-1)
    gate_half = gate_weight.astype(jnp.bfloat16)
    up_half = up_weight.astype(jnp.bfloat16)
    gate_full, up_full = (
        lax.all_gather(gate_half, "fs", axis=0, tiled=True),
        lax.all_gather(up_half, "fs", axis=0, tiled=True),
    )
    gate_acc = jnp.dot(inputs, gate_full, preferred_element_type=jnp.float32)
    up_acc = jnp.dot(inputs, up_full, preferred_element_type=jnp.float32)
    gate_pre = (gate_acc * gate_columns).astype(jnp.bfloat16)
    up_pre = (up_acc * up_columns).astype(jnp.bfloat16)
    hidden = (jax.nn.silu(causal_taps(gate_pre, gate_taps)) * causal_taps(up_pre, up_taps)).astype(
        jnp.bfloat16
    )
    down_full = lax.all_gather(down_weight.astype(jnp.bfloat16), "fs", axis=1, tiled=True)
    down_grouped = down_full.reshape(down_full.shape[0], groups, -1)
    summed_rows = lax.psum_scatter(
        jnp.einsum("lf,fgc->clg", hidden, down_grouped, preferred_element_type=jnp.float32).astype(
            jnp.bfloat16
        ),
        "tp",
        scatter_dimension=0,
        tiled=True,
    ).astype(jnp.float32)
    summed = jnp.transpose(summed_rows, (1, 2, 0))
    layer_out = (summed * down_scale + middle_values).astype(jnp.bfloat16)
    return layer_out[None]


def solution(mesh):
    placed = (
        P(("rep", "fs"), None, None, "tp"),
        P(None, "tp"),
        P(None, "fs", "tp"),
        P(None, "tp"),
        P(None, "tp"),
        P("fs", "tp"),
        P("fs", "tp"),
        P("fs", "tp"),
        P("fs", "tp"),
        P(None, "tp"),
        P(None, "tp"),
        P("tp", "fs"),
        P(None, "tp"),
    )
    return jax.shard_map(
        shards,
        mesh=mesh,
        in_specs=placed,
        out_specs=P(("rep", "fs"), None, None, "tp"),
        check_vma=False,
    )
```

profile of v0, /device:TPU:0, one launch (start us, length us, event | category | flops | bytes accessed | tf_op | source)
XLA Modules:
  0.0 510.5 jit_solution(17898336373341118964)
XLA Ops:
  6.5 0.0 all-gather.8.cloned.1.call-start
  6.6 1.4 fusion.10
  8.0 8.4 %psum.14 = f32[768,1,1]{0,2,1:T(1,128)S(1)} all-reduce(f32[768,1,1]{0,2,1:T(1,128)S(1)} %broadcast_in_dim.6), channel_id=1, replica_groups=mesh['rep'=2,'fs'=4,'tp'=4] {'tp'}, use_global_device_ids=true, to_apply=%region_1.0 | all-reduce | flops 768 | bytes 6144 | tf_op jit(solution)/shard_map/psum | solution.py:65
  16.4 1.4 fusion.14
  17.8 0.0 copy-done
  17.8 0.0 copy-done.7
  17.8 0.4 pad_add_fusion.2
  18.2 0.2 pad_add_fusion.1
  18.4 0.2 pad_add_fusion
  18.6 0.1 slice.97
  18.7 0.0 copy-start.4
  18.7 0.0 copy-start.12
  18.7 0.5 fusion.18
  19.2 1.0 pad_maximum_fusion
  20.2 0.0 all-gather.8.cloned.1.call-update
  20.2 0.0 all-gather.10.cloned.1.call-start
  20.3 0.1 copy.26
  20.4 14.7 %all_gather.25 = bf16[4,512,128]{1,2,0:T(8,128)(2,1)S(1)} all-gather(bf16[4,128,128]{1,2,0:T(8,128)(2,1)S(1)} %copy.26), channel_id=1, replica_groups=mesh['rep'=2,'fs'=4,'tp'=4] {'fs'}, dimensions={1}, use_global_device_ids=true | all-gather | bytes 655360 | tf_op jit(solution)/shard_map/all_gather | solution.py:63
  35.1 14.5 %all-gather.8.cloned.1.call-done = bf16[768,4,512]{2,0,1:T(8,128)(2,1)} async-done(((bf16[768,4,128]{2,0,1:T(8,128)(2,1)}), bf16[768,4,512]{2,0,1:T(8,128)(2,1)}) %all-gather.8.cloned.1.call-update) | async-done | bytes 3145744 | tf_op jit(solution)/shard_map/all_gather | solution.py:69
  49.6 2.9 fusion.6
  52.5 0.0 copy-start.2
  52.5 5.9 %psum.15 = f32[768,1,1]{0,2,1:T(1,128)S(1)} all-reduce(f32[768,1,1]{0,2,1:T(1,128)S(1)} %broadcast_in_dim.7), channel_id=1, replica_groups=mesh['rep'=2,'fs'=4,'tp'=4] {'tp'}, use_global_device_ids=true, to_apply=%region_3.0 | all-reduce | flops 768 | bytes 6144 | tf_op jit(solution)/shard_map/psum | solution.py:75
  58.5 0.0 copy-done.8
  58.5 1.2 fusion.8
  59.6 0.0 all-gather.10.cloned.1.call-update
  59.7 0.0 copy-start.1
  59.7 0.0 all-gather.14.cloned.1.call-start
  59.7 3.4 convert_element_type.93
  63.1 0.0 all-gather.14.cloned.1.call-update
  63.2 0.0 all-gather.12.cloned.1.call-start
  63.2 1.4 convert_element_type.90
  64.6 0.0 all-gather.12.cloned.1.call-update
  64.7 0.0 copy-start.10
  64.7 0.0 copy-start.11
  64.7 0.0 copy-start.5
  64.7 0.0 copy-start.6
  64.7 0.0 all-gather.16.cloned.1.call-start
  64.8 3.1 copy.29
  67.8 0.0 all-gather.16.cloned.1.call-update
  67.8 0.0 reduce-scatter.4.cloned.1.call-start
  67.9 0.0 copy-done.10
  67.9 12.1 %all-gather.1 = f32[4,1,384]{2,1,0:T(1,128)S(1)} all-gather(f32[1,1,384]{2,1,0:T(1,128)S(1)} %bitcast.55), channel_id=1, replica_groups=mesh['rep'=2,'fs'=4,'tp'=4] {'fs'}, dimensions={0}, use_global_device_ids=true | all-gather | bytes 7680 | tf_op jit(solution)/shard_map/all_gather | solution.py:80
  80.1 12.1 %all-gather = f32[4,1,384]{2,1,0:T(1,128)S(1)} all-gather(f32[1,1,384]{2,1,0:T(1,128)S(1)} %bitcast.56), channel_id=1, replica_groups=mesh['rep'=2,'fs'=4,'tp'=4] {'fs'}, dimensions={0}, use_global_device_ids=true | all-gather | bytes 7680 | tf_op jit(solution)/shard_map/all_gather | solution.py:79
  92.2 0.0 copy-done.5
  92.2 0.0 copy-done.6
  92.2 0.1 slice_reduce_fusion.2
  92.3 0.0 all-gather.10.cloned.1.call-done
  92.4 3.2 copy.28
  95.6 111.2 %all-gather.14.cloned.1.call-done = bf16[2048,1536]{1,0:T(8,128)(2,1)} async-done(((bf16[512,1536]{1,0:T(8,128)(2,1)}), bf16[2048,1536]{1,0:T(8,128)(2,1)}) %all-gather.14.cloned.1.call-update) | async-done | bytes 6291472 | tf_op jit(solution)/shard_map/all_gather | solution.py:88
  206.7 9.5 %fusion.1 = f32[768,1536]{1,0:T(8,128)} fusion(bf16[768,2048]{0,1:T(8,128)(2,1)S(1)} %bitcast.52, bf16[2048,1536]{1,0:T(8,128)(2,1)} %all-gather.14.cloned.1.call-done, f32[1536]{0:T(1024)S(1)} %mul.178), kind=kOutput, calls=%fused_computation.4 | convolution fusion | flops 4835377152 | bytes 14161920 | tf_op jit(solution)/shard_map/dot_general | solution.py:91
  216.3 105.4 %all-gather.12.cloned.1.call-done = bf16[2048,1536]{1,0:T(8,128)(2,1)} async-done(((bf16[512,1536]{1,0:T(8,128)(2,1)}), bf16[2048,1536]{1,0:T(8,128)(2,1)}) %all-gather.12.cloned.1.call-update) | async-done | bytes 6291472 | tf_op jit(solution)/shard_map/all_gather | solution.py:87
  321.7 9.5 %fusion = f32[768,1536]{1,0:T(8,128)} fusion(bf16[768,2048]{0,1:T(8,128)(2,1)S(1)} %bitcast.53, bf16[2048,1536]{1,0:T(8,128)(2,1)} %all-gather.12.cloned.1.call-done, f32[1536]{0:T(1024)S(1)} %mul.165), kind=kOutput, calls=%fused_computation.3 | convolution fusion | flops 4835377152 | bytes 14161920 | tf_op jit(solution)/shard_map/dot_general | solution.py:90
  331.2 105.5 %all-gather.16.cloned.1.call-done = bf16[1536,2048]{0,1:T(8,128)(2,1)} async-done(((bf16[1536,512]{0,1:T(8,128)(2,1)}), bf16[1536,2048]{0,1:T(8,128)(2,1)}) %all-gather.16.cloned.1.call-update) | async-done | bytes 6291472 | tf_op jit(solution)/shard_map/all_gather | solution.py:97
  436.7 19.3 %convert_bitcast_fusion = bf16[512,768,4]{0,1,2:T(8,128)(2,1)} fusion(bf16[1536,4,512]{0,2,1:T(8,128)(2,1)} %bitcast.57, f32[766,1536]{1,0:T(8,128)} %bitcast.58, f32[1536]{0:T(1024)S(1)} %get-tuple-element.9, f32[767,1536]{1,0:T(8,128)} %bitcast.59, f32[1536]{0:T(1024)S(1)} %get-tuple-element.10, f32[768,1536]{1,0:T(8,128)} %fusion.1, ...), kind=kOutput, calls=%fused_computation.5 | convolution fusion | flops 4852285440 | bytes 37748736 | tf_op jit(solution)/shard_map/lf,fgc->clg/dot_general | solution.py:100
  455.9 4.7 copy.34
  460.6 2.4 copy.36
  463.0 0.0 reduce-scatter.4.cloned.1.call-update
  463.0 36.2 %reduce-scatter.4.cloned.1.call-done = bf16[128,3072]{1,0:T(8,128)(2,1)} async-done(((bf16[512,3072]{1,0:T(8,128)(2,1)}), bf16[128,3072]{1,0:T(8,128)(2,1)}) %reduce-scatter.4.cloned.1.call-update) | async-done | bytes 786448
  499.2 2.0 reshape.64
  501.2 0.7 copy.35
  501.9 0.0 copy-done.3
  501.9 0.0 copy-done.9
  501.9 0.3 fusion.15
  502.2 1.5 copy.31
  (20 shorter events, 0.2 us)
Async XLA Ops:
  6.5 11.3 %copy-start = (bf16[1,768,4,128]{3,2,1,0:T(4,128)(2,1)S(1)}, bf16[1,768,4,128]{3,2,1,0:T(4,128)(2,1)}, u32[]{:S(2)}) copy-start(bf16[1,768,4,128]{3,2,1,0:T(4,128)(2,1)} %param.13) | copy-start | bytes 2359300
  6.5 11.3 %copy-start.7 = (f32[4,128]{1,0:T(4,128)S(1)}, f32[4,128]{1,0:T(4,128)}, u32[]{:S(2)}) copy-start(f32[4,128]{1,0:T(4,128)} %param.14) | copy-start | bytes 6148
  6.5 43.0 %all-gather.8.cloned.1.call-start = ((), (), s32[]{:S(2)}) async-start(), calls=%async_computation.1 | async-start | bytes 3932160 | tf_op jit(solution)/shard_map/all_gather | solution.py:69
  18.7 1.6 copy-start.4
  18.7 30.9 %copy-start.12 = (f32[4,128]{1,0:T(4,128)S(1)}, f32[4,128]{1,0:T(4,128)}, u32[]{:S(2)}) copy-start(f32[4,128]{1,0:T(4,128)} %param.16) | copy-start | bytes 6148
  20.2 72.2 %all-gather.10.cloned.1.call-start = ((), (), s32[]{:S(2)}) async-start(), calls=%async_computation.2 | async-start | bytes 3932160 | tf_op jit(solution)/shard_map/all_gather | solution.py:77
  35.1 23.4 %copy-start.8 = (f32[4,128]{1,0:T(4,128)S(1)}, f32[4,128]{1,0:T(4,128)}, u32[]{:S(2)}) copy-start(f32[4,128]{1,0:T(4,128)} %param.17) | copy-start | bytes 6148
  52.5 7.1 %copy-start.2 = (bf16[768,4,128]{2,0,1:T(8,128)(2,1)}, bf16[768,4,128]{2,0,1:T(8,128)(2,1)S(1)}, u32[]{:S(2)}) copy-start(bf16[768,4,128]{2,0,1:T(8,128)(2,1)S(1)} %get-tuple-element.16) | copy-start | bytes 2359300
  59.7 3.6 copy-start.1
  59.7 147.0 %all-gather.14.cloned.1.call-start = ((), (), s32[]{:S(2)}) async-start(), calls=%async_computation.4 | async-start | bytes 7864320 | tf_op jit(solution)/shard_map/all_gather | solution.py:88
  63.2 258.5 %all-gather.12.cloned.1.call-start = ((), (), s32[]{:S(2)}) async-start(), calls=%async_computation.3 | async-start | bytes 7864320 | tf_op jit(solution)/shard_map/all_gather | solution.py:87
  64.7 3.2 copy-start.10
  64.7 15.4 %copy-start.11 = (f32[1,384]{1,0:T(1,128)S(1)}, f32[1,384]{1,0:T(1,128)}, u32[]{:S(2)}) copy-start(f32[1,384]{1,0:T(1,128)} %param.20) | copy-start | bytes 4612
  64.7 27.5 %copy-start.5 = (f32[3,1536]{1,0:T(4,128)S(1)}, f32[3,1536]{1,0:T(4,128)}, u32[]{:S(2)}) copy-start(f32[3,1536]{1,0:T(4,128)} %param.23) | copy-start | bytes 55300
  64.7 27.5 %copy-start.6 = (f32[3,1536]{1,0:T(4,128)S(1)}, f32[3,1536]{1,0:T(4,128)}, u32[]{:S(2)}) copy-start(f32[3,1536]{1,0:T(4,128)} %param.22) | copy-start | bytes 55300
  64.7 371.9 %all-gather.16.cloned.1.call-start = ((), (), s32[]{:S(2)}) async-start(), calls=%async_computation.5 | async-start | bytes 7864320 | tf_op jit(solution)/shard_map/all_gather | solution.py:97
  67.8 431.4 %reduce-scatter.4.cloned.1.call-start = ((), (), s32[]{:S(2)}) async-start(), calls=%async_computation.6 | async-start | bytes 3932160
  463.0 38.9 %copy-start.3 = (bf16[768,4,128]{2,0,1:T(8,128)(2,1)S(1)}, bf16[768,4,128]{2,0,1:T(8,128)(2,1)}, u32[]{:S(2)}) copy-start(bf16[768,4,128]{2,0,1:T(8,128)(2,1)} %copy-done.2) | copy-start | bytes 2359300
  463.0 38.9 %copy-start.9 = (f32[4,128]{1,0:T(4,128)S(1)}, f32[4,128]{1,0:T(4,128)}, u32[]{:S(2)}) copy-start(f32[4,128]{1,0:T(4,128)} %param.25) | copy-start | bytes 6148
Sparse Core Ops, SparseCore 0:
  20.3 29.1 all-gather.7
  59.8 29.9 all-gather.9
  91.4 115.3 all-gather.13
  208.1 113.5 all-gather.11
  323.1 113.5 all-gather.15
  463.1 36.0 reduce-scatter.3
where the time goes:
time: 511 us
  waiting for transfers between devices  373 us (73%)
  blocking collectives  53.2 us (10%)
  matrix products  41.2 us (8%)
  local copies, waits for them, and re-layouts  17.9 us (4%)
  between operations  13.8 us (3%)
  other arithmetic  11.3 us (2%)
    all_gather x1, waiting for transfers between devices, shards(): lax.all_gather(up_half, 'fs', axis=0, tiled=True)  111 us
    all_gather x1, waiting for transfers between devices, shards(): lax.all_gather(down_weight.astype(jnp.bfloat16), 'fs', axis=1, tiled=True)  105 us
    all_gather x1, waiting for transfers between devices, shards(): lax.all_gather(gate_half, 'fs', axis=0, tiled=True)  105 us
    unnamed x7, waiting for transfers between devices  36.3 us
    dot_general x1, matrix products, shards(): jnp.einsum('lf,fgc->clg', hidden, down_grouped, preferred_element_type=jn...  19.3 us
    all_gather x1, blocking collectives, shards(): lax.all_gather(pool_weight.astype(jnp.bfloat16), 'fs', axis=1, tiled=True)  14.7 us
    all_gather x1, waiting for transfers between devices, shards(): lax.all_gather(pooled, 'tp', axis=2, tiled=True)  14.5 us
    unnamed x32, local copies, waits for them, and re-layouts  13 us
  transfers between devices with their start and end apart: 6, of which 5 were waited for; matrix products, arithmetic and copies ran while one was open for 6% of the time, Pallas kernels for 0%

commit v1 on v0

v1 whole, which is shorter than its diff:
```python
import functools

import jax
import jax.numpy as jnp
from jax import lax
from jax.experimental import pallas as pl
from jax.experimental.pallas import tpu as pltpu
from jax.sharding import PartitionSpec as P

WINDOWS = (2, 4, 8, 16)
EPSILON = 1e-05
SUBS = 2
COLUMNS = 256
F32 = jnp.float32
BF16 = jnp.bfloat16


def delayed(values, steps):
    rows = lax.broadcasted_iota(jnp.int32, values.shape, 0)
    return jnp.where(rows >= steps, pltpu.roll(values, steps, 0), 0.0)


def causal_taps(values, taps):
    return taps[2:3] * values + taps[1:2] * delayed(values, 1) + taps[0:1] * delayed(values, 2)


def block_kernel(
    sizes,
    residual,
    gains,
    pool_scale,
    down_scale,
    scale_pair,
    gate_taps,
    up_taps,
    pool_own,
    gate_own,
    up_own,
    down_own,
    out,
    pool_full,
    gate_full,
    up_full,
    down_full,
    gathered,
    middle_all,
    gains_all,
    scales_all,
    scale_row,
    pooled,
    middle,
    inputs,
    gate_pre,
    hidden,
    partials,
    arrived,
    ring_send,
    ring_recv,
    rep_send,
    rep_recv,
    pool_send,
    pool_recv,
    pool_rep_send,
    pool_rep_recv,
    scale_send,
    scale_recv,
    tp_send,
    tp_recv,
    part_send,
    part_recv,
    local_sem,
):
    n_rep, n_fs, n_tp = sizes
    rep, fs, tp = (lax.axis_index(name) for name in ("rep", "fs", "tp"))
    length = residual.shape[0]
    groups = pool_full.shape[0]
    channels = pool_full.shape[1]
    local = residual.shape[1] // groups
    width = groups * channels

    def other(axis, offset):
        me, count = {"rep": (rep, n_rep), "fs": (fs, n_fs), "tp": (tp, n_tp)}[axis]
        return lax.rem(me + offset, count)

    def remote(src, dst, send, recv, axis, offset):
        return pltpu.make_async_remote_copy(
            src_ref=src,
            dst_ref=dst,
            send_sem=send,
            recv_sem=recv,
            device_id={axis: other(axis, offset)},
            device_id_type=pl.DeviceIdType.MESH,
        )

    barrier = pltpu.get_barrier_semaphore()
    for axis, count in (("rep", n_rep), ("fs", n_fs), ("tp", n_tp)):
        for offset in range(1, count):
            pl.semaphore_signal(
                barrier,
                inc=1,
                device_id={axis: other(axis, offset)},
                device_id_type=pl.DeviceIdType.MESH,
            )
    pl.semaphore_wait(barrier, n_rep + n_fs + n_tp - 3)

    sent = []

    def start(copy):
        copy.start()
        sent.append(copy)

    weights = ((gate_own, gate_full), (up_own, up_full), (down_own, down_full))

    def piece(w, shard, half, sub, own=False):
        rows = weights[w][0].shape[0] // (n_rep * SUBS)
        part = pl.ds(pl.multiple_of((half * SUBS + sub) * rows, rows), rows)
        return weights[w][0].at[part] if own else weights[w][1].at[shard, part]

    def ring(w, sub, step):
        shard = lax.rem(fs - step + n_fs, n_fs)
        return remote(
            piece(w, shard, rep, sub, own=step == 0),
            piece(w, shard, rep, sub),
            ring_send.at[w, sub, step],
            ring_recv.at[w, sub, step],
            "fs",
            1,
        )

    def serve(w, sub, step):
        shard = lax.rem(fs - step - 1 + n_fs, n_fs)
        mine = piece(w, shard, rep, sub)
        remote(
            mine, mine, ring_send.at[w, sub, step], ring_recv.at[w, sub, step], "fs", 1
        ).wait_recv()
        for d in range(1, n_rep):
            start(
                remote(
                    mine,
                    mine,
                    rep_send.at[w, sub, step, d - 1],
                    rep_recv.at[w, sub, step, d - 1],
                    "rep",
                    d,
                )
            )
        if step < n_fs - 2:
            start(ring(w, sub, step + 1))

    def settle(w, step):
        shard = lax.rem(fs - step - 1 + n_fs, n_fs)
        for sub in range(SUBS):
            for d in range(1, n_rep):
                got = piece(w, shard, other("rep", n_rep - d), sub)
                remote(
                    got,
                    got,
                    rep_send.at[w, sub, step, d - 1],
                    rep_recv.at[w, sub, step, d - 1],
                    "rep",
                    d,
                ).wait_recv()

    def local_copy(src, dst, idx):
        copy = pltpu.make_async_copy(src, dst, local_sem.at[idx])
        copy.start()
        return copy

    own_copies = [
        local_copy(residual, gathered.at[tp], 0),
        local_copy(gains, gains_all.at[tp], 1),
        local_copy(scale_pair, scales_all.at[fs], 2),
        local_copy(gate_own, gate_full.at[fs], 3),
        local_copy(up_own, up_full.at[fs], 4),
        local_copy(down_own, down_full.at[fs], 5),
    ]

    pool_rows = pool_own.shape[1]
    rep_groups = groups // n_rep

    def pool_part(shard, half):
        return pool_full.at[
            pl.ds(half * rep_groups, rep_groups),
            pl.ds(pl.multiple_of(shard * pool_rows, pool_rows), pool_rows),
        ]

    pool_copy = local_copy(
        pool_own, pool_full.at[:, pl.ds(pl.multiple_of(fs * pool_rows, pool_rows), pool_rows)], 6
    )

    for d in range(1, n_fs):
        start(
            remote(
                pool_own.at[pl.ds(rep * rep_groups, rep_groups)],
                pool_part(fs, rep),
                pool_send.at[d - 1],
                pool_recv.at[d - 1],
                "fs",
                d,
            )
        )
    for w in (0, 1):
        for sub in range(SUBS):
            if n_fs > 1:
                start(ring(w, sub, 0))
    for d in range(1, n_tp):
        start(remote(gains, gains_all.at[tp], tp_send.at[0, d - 1], tp_recv.at[0, d - 1], "tp", d))
    for d in range(1, n_tp):
        start(
            remote(residual, gathered.at[tp], tp_send.at[1, d - 1], tp_recv.at[1, d - 1], "tp", d)
        )
    for d in range(1, n_fs):
        start(
            remote(
                scale_pair, scales_all.at[fs], scale_send.at[d - 1], scale_recv.at[d - 1], "fs", d
            )
        )

    for d in range(1, n_fs):
        shard = other("fs", n_fs - d)
        mine = pool_part(shard, rep)
        remote(mine, mine, pool_send.at[d - 1], pool_recv.at[d - 1], "fs", d).wait_recv()
        for e in range(1, n_rep):
            start(
                remote(
                    mine,
                    mine,
                    pool_rep_send.at[d - 1, e - 1],
                    pool_rep_recv.at[d - 1, e - 1],
                    "rep",
                    e,
                )
            )
    for d in range(1, n_fs):
        shard = other("fs", n_fs - d)
        for e in range(1, n_rep):
            got = pool_part(shard, other("rep", n_rep - e))
            remote(
                got,
                got,
                pool_rep_send.at[d - 1, e - 1],
                pool_rep_recv.at[d - 1, e - 1],
                "rep",
                e,
            ).wait_recv()
    pool_copy.wait()
    for copy in own_copies:
        copy.wait()

    def tp_arrivals(idx, buffer):
        for d in range(1, n_tp):
            got = buffer.at[other("tp", n_tp - d)]
            remote(got, got, tp_send.at[idx, d - 1], tp_recv.at[idx, d - 1], "tp", d).wait_recv()

    for sub in range(SUBS):
        serve(0, sub, 0)
    tp_arrivals(0, gains_all)
    tp_arrivals(1, gathered)
    for sub in range(SUBS):
        serve(1, sub, 0)

    def mean_square_root(buffer):
        total = jnp.zeros((length, 1), F32)
        for t in range(n_tp):
            values = buffer[t].astype(F32)
            total = total + jnp.sum(values * values, axis=1, keepdims=True)
        return lax.rsqrt(total / width + EPSILON)

    factor = mean_square_root(gathered)
    positions = lax.broadcasted_iota(jnp.int32, (length, 1), 0).astype(F32) + 1.0
    for g in range(groups):
        part = slice(g * local, (g + 1) * local)
        share = 1.0 / jnp.minimum(positions, float(WINDOWS[g]))
        for t in range(n_tp):
            values = gathered[t, :, part].astype(F32)
            normed = (values * factor * gains_all[t, 0:1, part]).astype(BF16).astype(F32)
            totals = normed
            reach = 1
            while reach < WINDOWS[g]:
                totals = totals + delayed(totals, reach)
                reach = reach * 2
            pooled[:, t * local : (t + 1) * local] = (totals * share - normed).astype(BF16)
        mixed = jnp.dot(pooled[...], pool_full[g], preferred_element_type=F32)
        middle[:, part] = (
            mixed * pool_scale[:, part] + residual[:, part].astype(F32)
        ).astype(BF16)

    middle_copy = local_copy(middle, middle_all.at[tp], 0)
    for d in range(1, n_tp):
        start(
            remote(middle, middle_all.at[tp], tp_send.at[2, d - 1], tp_recv.at[2, d - 1], "tp", d)
        )
    for step in range(1, n_fs - 1):
        for w in (0, 1):
            if step == n_fs - 2 and n_fs > 2:
                break
            for sub in range(SUBS):
                serve(w, sub, step)
    for sub in range(SUBS):
        if n_fs > 1:
            start(ring(2, sub, 0))
    for d in range(1, n_fs):
        got = scales_all.at[other("fs", n_fs - d)]
        remote(got, got, scale_send.at[d - 1], scale_recv.at[d - 1], "fs", d).wait_recv()
    shard_columns = scale_pair.shape[1]
    for f in range(n_fs):
        scale_row[:, f * shard_columns : (f + 1) * shard_columns] = scales_all[f]

    middle_copy.wait()
    tp_arrivals(2, middle_all)
    factor = mean_square_root(middle_all)
    for t in range(n_tp):
        for g in range(groups):
            part = slice(g * local, (g + 1) * local)
            start_column = g * channels + t * local
            inputs[:, start_column : start_column + local] = (
                middle_all[t, :, part].astype(F32) * factor * gains_all[t, 1:2, part]
            ).astype(BF16)

    def finish(w):
        if n_fs > 2:
            for sub in range(SUBS):
                serve(w, sub, n_fs - 2)
        for step in range(n_fs - 1):
            settle(w, step)

    def product(full, columns, row):
        block = full[:, :, columns].reshape(width, COLUMNS)
        made = jnp.dot(inputs[...], block, preferred_element_type=F32)
        return (made * scale_row[row : row + 1, columns]).astype(BF16)

    chunks = gate_full.shape[2] // COLUMNS

    finish(0)

    @pl.loop(0, chunks)
    def _(j):
        columns = pl.ds(pl.multiple_of(j * COLUMNS, COLUMNS), COLUMNS)
        gate_pre[:, columns] = product(gate_full, columns, 0)

    finish(1)
    for sub in range(SUBS):
        if n_fs > 1:
            serve(2, sub, 0)

    @pl.loop(0, chunks)
    def _(j):
        columns = pl.ds(pl.multiple_of(j * COLUMNS, COLUMNS), COLUMNS)
        up_values = product(up_full, columns, 1).astype(F32)
        conv_gate = causal_taps(gate_pre[:, columns].astype(F32), gate_taps[:, columns])
        conv_up = causal_taps(up_values, up_taps[:, columns])
        silu = conv_gate / (1.0 + jnp.exp(-conv_gate))
        hidden[:, columns] = (silu * conv_up).astype(BF16)

    shard_width = down_own.shape[1]

    def to_peers(idx, src, dst):
        for d in range(1, n_tp):
            start(
                remote(
                    src(other("tp", d)),
                    dst(tp),
                    part_send.at[idx, d - 1],
                    part_recv.at[idx, d - 1],
                    "tp",
                    d,
                )
            )

    def from_peers(idx, dst):
        for d in range(1, n_tp):
            got = dst(other("tp", n_tp - d))
            remote(
                got, got, part_send.at[idx, d - 1], part_recv.at[idx, d - 1], "tp", d
            ).wait_recv()

    def conclude(g, columns):
        total = partials[tp, g].astype(F32)
        for d in range(1, n_tp):
            total = total + arrived[other("tp", d), g].astype(F32)
        out[:, columns] = (
            total * down_scale[:, columns] + middle[:, columns].astype(F32)
        ).astype(BF16)

    if shard_width == channels and local % 128 == 0:
        for step in range(n_fs):
            shard = lax.rem(fs - step + n_fs, n_fs)
            if step >= 1:
                if step >= 2:
                    for sub in range(SUBS):
                        serve(2, sub, step - 1)
                settle(2, step - 1)
            made = jnp.dot(hidden[...], down_full[shard], preferred_element_type=F32)
            for t in range(n_tp):
                partials[t, shard] = made[:, t * local : (t + 1) * local].astype(BF16)
            to_peers(step, lambda t: partials.at[t, shard], lambda t: arrived.at[t, shard])
        for step in range(n_fs):
            shard = lax.rem(fs - step + n_fs, n_fs)
            from_peers(step, lambda t: arrived.at[t, shard])
            conclude(shard, pl.ds(pl.multiple_of(shard * local, local), local))
    else:
        for step in range(n_fs - 1):
            if step >= 1:
                for sub in range(SUBS):
                    serve(2, sub, step)
            settle(2, step)
        for f in range(n_fs):
            made = jnp.dot(hidden[...], down_full[f], preferred_element_type=F32).astype(BF16)
            span = min(local, shard_width)
            for at in range(0, shard_width, span):
                g, channel = divmod(f * shard_width + at, channels)
                t, low = divmod(channel, local)
                partials[t, g, :, low : low + span] = made[:, at : at + span]
        to_peers(0, lambda t: partials.at[t], lambda t: arrived.at[t])
        from_peers(0, lambda t: arrived.at[t])
        for g in range(groups):
            conclude(g, slice(g * local, (g + 1) * local))

    for copy in sent:
        copy.wait_send()


def shards(
    sizes,
    residual,
    mixer_gain,
    pool_weight,
    pool_scale,
    channel_gain,
    gate_weight,
    up_weight,
    gate_scale,
    up_scale,
    gate_taps,
    up_taps,
    down_weight,
    down_scale,
):
    n_rep, n_fs, n_tp = sizes
    _, length, groups, local = residual.shape
    channels = local * n_tp
    width = groups * channels
    own_width = groups * local
    hidden_width = gate_weight.shape[1]
    vmem = pl.BlockSpec(memory_space=pltpu.VMEM)
    anywhere = pl.BlockSpec(memory_space=pl.ANY)
    dma = pltpu.SemaphoreType.DMA
    hops = max(n_fs - 1, 1)
    reps = max(n_rep - 1, 1)
    peers = max(n_tp - 1, 1)
    out = pl.pallas_call(
        functools.partial(block_kernel, sizes),
        out_shape=jax.ShapeDtypeStruct((length, own_width), BF16),
        in_specs=[vmem] * 8 + [anywhere] * 3,
        out_specs=vmem,
        scratch_shapes=[
            pltpu.VMEM((groups, channels, local), BF16),
            pltpu.VMEM((n_fs,) + gate_weight.shape, BF16),
            pltpu.VMEM((n_fs,) + up_weight.shape, BF16),
            pltpu.VMEM((n_fs,) + down_weight.shape, BF16),
            pltpu.VMEM((n_tp, length, own_width), BF16),
            pltpu.VMEM((n_tp, length, own_width), BF16),
            pltpu.VMEM((n_tp, 2, own_width), F32),
            pltpu.VMEM((n_fs, 2, gate_scale.shape[1]), F32),
            pltpu.VMEM((2, hidden_width), F32),
            pltpu.VMEM((length, channels), BF16),
            pltpu.VMEM((length, own_width), BF16),
            pltpu.VMEM((length, width), BF16),
            pltpu.VMEM((length, hidden_width), BF16),
            pltpu.VMEM((length, hidden_width), BF16),
            pltpu.VMEM((n_tp, groups, length, local), BF16),
            pltpu.VMEM((n_tp, groups, length, local), BF16),
            dma((3, SUBS, hops)),
            dma((3, SUBS, hops)),
            dma((3, SUBS, hops, reps)),
            dma((3, SUBS, hops, reps)),
            dma((hops,)),
            dma((hops,)),
            dma((hops, reps)),
            dma((hops, reps)),
            dma((hops,)),
            dma((hops,)),
            dma((3, peers)),
            dma((3, peers)),
            dma((n_fs, peers)),
            dma((n_fs, peers)),
            dma((7,)),
        ],
        compiler_params=pltpu.CompilerParams(
            collective_id=0, has_side_effects=True, vmem_limit_bytes=60 * 1024 * 1024
        ),
    )(
        residual.reshape(length, own_width),
        jnp.stack([mixer_gain.reshape(-1), channel_gain.reshape(-1)]),
        pool_scale.reshape(1, -1),
        down_scale.reshape(1, -1),
        jnp.concatenate([gate_scale, up_scale], axis=0),
        gate_taps,
        up_taps,
        pool_weight.astype(BF16),
        gate_weight.astype(BF16),
        up_weight.astype(BF16),
        down_weight.astype(BF16),
    )
    return out.reshape(1, length, groups, local)


def solution(mesh):
    placed = (
        P(("rep", "fs"), None, None, "tp"),
        P(None, "tp"),
        P(None, "fs", "tp"),
        P(None, "tp"),
        P(None, "tp"),
        P("fs", "tp"),
        P("fs", "tp"),
        P("fs", "tp"),
        P("fs", "tp"),
        P(None, "tp"),
        P(None, "tp"),
        P("tp", "fs"),
        P(None, "tp"),
    )
    sizes = tuple(mesh.shape[name] for name in ("rep", "fs", "tp"))
    return jax.shard_map(
        functools.partial(shards, sizes),
        mesh=mesh,
        in_specs=placed,
        out_specs=P(("rep", "fs"), None, None, "tp"),
        check_vma=False,
    )
```

time: 511 us -> 317 us (0.62)
  the two profiles are of different devices: /device:TPU:0 before, /device:TPU:11 now
where the time goes in v1:
time: 317 us
  Pallas kernels  301 us (95%)
  other arithmetic  10.1 us (3%)
  local copies, waits for them, and re-layouts  5.87 us (2%)
    pallas_call x1, Pallas kernels, shards(): pl.pallas_call(functools.partial(block_kernel, sizes), out_shape=jax.Shap...  301 us

profile of v1, /device:TPU:11, one launch (start us, length us, event | category | flops | bytes accessed | tf_op | source)
XLA Modules:
  0.0 317.2 jit_solution(6953499702105570309)
XLA Ops:
  0.0 1.3 pad_maximum_fusion.1.scale_pair
  1.3 1.3 pad_maximum_fusion.gains
  2.6 1.6 convert_element_type.12.pool_own
  4.2 0.0 copy-start
  4.2 2.3 copy.16
  6.5 3.2 %convert_element_type.13.gate_own = bf16[512,1536]{1,0:T(8,128)(2,1)} convert(f32[512,1536]{1,0:T(8,128)} %param.18) | non-fusion elementwise | flops 786432 | bytes 4718592 | tf_op jit(solution)/shard_map/convert_element_type | solution.py:501
  9.7 0.0 copy-done
  9.7 0.0 copy-start.1
  9.7 1.3 convert_element_type.14.up_own
  11.1 1.1 copy-done.1
  12.2 1.3 convert_element_type.15.down_own
  13.5 301.2 %shard_map.127 = bf16[768,512]{1,0:T(8,128)(2,1)} custom-call(bf16[768,512]{1,0:T(8,128)(2,1)} %bitcast.9, f32[2,512]{1,0:T(2,128)} %pad_maximum_fusion.gains, f32[1,512]{1,0:T(1,128)} %bitcast.11, f32[1,512]{1,0:T(1,128)} %bitcast.12, f32[2,384]{1,0:T(2,128)} %pad_maximum_fusion.1.scale_pair, f32[3,1536]{1,0:T(4,128)} %gate_taps.1, f32[3,1536]{1,0:T(4,128)} %up_taps.1, ...), custom_call_target="tpu_custom_call" | custom-call | tf_op jit(solution)/shard_map/pallas_call | solution.py:451
  314.7 2.4 reshape.15
Async XLA Ops:
  4.2 5.5 %copy-start = (f32[512,1536]{1,0:T(8,128)S(1)}, f32[512,1536]{1,0:T(8,128)}, u32[]{:S(2)}) copy-start(f32[512,1536]{1,0:T(8,128)} %param.19) | copy-start | bytes 9437188
  9.7 2.5 copy-start.1

commit v2 on v1

--- a/solution.py
+++ b/solution.py
@@ -105,9 +105,12 @@
 
     sent = []
 
-    def start(copy):
-        copy.start()
-        sent.append(copy)
+    def start(copy, valid=None):
+        sent.append((copy, valid))
+        if valid is None:
+            copy.start()
+        else:
+            pl.when(valid)(copy.start)
 
     weights = ((gate_own, gate_full), (up_own, up_full), (down_own, down_full))
 
@@ -116,50 +119,74 @@
         part = pl.ds(pl.multiple_of((half * SUBS + sub) * rows, rows), rows)
         return weights[w][0].at[part] if own else weights[w][1].at[shard, part]
 
-    def ring(w, sub, step):
-        shard = lax.rem(fs - step + n_fs, n_fs)
-        return remote(
-            piece(w, shard, rep, sub, own=step == 0),
-            piece(w, shard, rep, sub),
-            ring_send.at[w, sub, step],
-            ring_recv.at[w, sub, step],
-            "fs",
-            1,
-        )
-
-    def serve(w, sub, step):
-        shard = lax.rem(fs - step - 1 + n_fs, n_fs)
-        mine = piece(w, shard, rep, sub)
-        remote(
-            mine, mine, ring_send.at[w, sub, step], ring_recv.at[w, sub, step], "fs", 1
-        ).wait_recv()
-        for d in range(1, n_rep):
+    def shard_sent(step, way):
+        shard = fs + step if way else fs - step
+        return jnp.clip(shard, 0, n_fs - 1), (shard <= n_fs - 1 if way else shard >= 0)
+
+    def line(w, sub, step):
+        for way in range(2):
+            shard, valid = shard_sent(step, way)
             start(
                 remote(
-                    mine,
-                    mine,
-                    rep_send.at[w, sub, step, d - 1],
-                    rep_recv.at[w, sub, step, d - 1],
-                    "rep",
-                    d,
+                    piece(w, shard, rep, sub, own=step == 0),
+                    piece(w, shard, rep, sub),
+                    ring_send.at[w, sub, 2 * step + way],
+                    ring_recv.at[w, sub, 2 * step + way],
+                    "fs",
+                    n_fs - 1 if way else 1,
+                ),
+                valid & (fs > 0 if way else fs < n_fs - 1),
+            )
+
+    def serve(w, sub, step):
+        for way in range(2):
+            shard, valid = shard_sent(step + 1, way)
+            mine = piece(w, shard, rep, sub)
+            sems = (w, sub, 2 * step + way)
+            pl.when(valid)(
+                remote(
+                    mine, mine, ring_send.at[sems], ring_recv.at[sems], "fs", 1
+                ).wait_recv
+            )
+            if step < n_fs - 2:
+                onward = (w, sub, 2 * step + 2 + way)
+                start(
+                    remote(
+                        mine,
+                        mine,
+                        ring_send.at[onward],
+                        ring_recv.at[onward],
+                        "fs",
+                        n_fs - 1 if way else 1,
+                    ),
+                    valid & (fs > 0 if way else fs < n_fs - 1),
                 )
-            )
-        if step < n_fs - 2:
-            start(ring(w, sub, step + 1))
-
-    def settle(w, step):
-        shard = lax.rem(fs - step - 1 + n_fs, n_fs)
-        for sub in range(SUBS):
             for d in range(1, n_rep):
-                got = piece(w, shard, other("rep", n_rep - d), sub)
-                remote(
-                    got,
-                    got,
-                    rep_send.at[w, sub, step, d - 1],
-                    rep_recv.at[w, sub, step, d - 1],
-                    "rep",
-                    d,
-                ).wait_recv()
+                start(
+                    remote(
+                        mine,
+                        mine,
+                        rep_send.at[sems + (d - 1,)],
+                        rep_recv.at[sems + (d - 1,)],
+                        "rep",
+                        d,
+                    ),
+                    valid,
+                )
+
+    def settle(w, step, ways=(0, 1)):
+        for way in ways:
+            shard, valid = shard_sent(step + 1, way)
+
+            @pl.when(valid)
+            def _():
+                for sub in range(SUBS):
+                    for d in range(1, n_rep):
+                        got = piece(w, shard, other("rep", n_rep - d), sub)
+                        sems = (w, sub, 2 * step + way, d - 1)
+                        remote(
+                            got, got, rep_send.at[sems], rep_recv.at[sems], "rep", d
+                        ).wait_recv()
 
     def local_copy(src, dst, idx):
         copy = pltpu.make_async_copy(src, dst, local_sem.at[idx])
@@ -202,7 +229,7 @@
     for w in (0, 1):
         for sub in range(SUBS):
             if n_fs > 1:
-                start(ring(w, sub, 0))
+                line(w, sub, 0)
     for d in range(1, n_tp):
         start(remote(gains, gains_all.at[tp], tp_send.at[0, d - 1], tp_recv.at[0, d - 1], "tp", d))
     for d in range(1, n_tp):
@@ -298,7 +325,7 @@
                 serve(w, sub, step)
     for sub in range(SUBS):
         if n_fs > 1:
-            start(ring(2, sub, 0))
+            line(2, sub, 0)
     for d in range(1, n_fs):
         got = scales_all.at[other("fs", n_fs - d)]
         remote(got, got, scale_send.at[d - 1], scale_recv.at[d - 1], "fs", d).wait_recv()
@@ -383,21 +410,38 @@
         ).astype(BF16)
 
     if shard_width == channels and local % 128 == 0:
-        for step in range(n_fs):
-            shard = lax.rem(fs - step + n_fs, n_fs)
-            if step >= 1:
-                if step >= 2:
-                    for sub in range(SUBS):
-                        serve(2, sub, step - 1)
-                settle(2, step - 1)
+        def share(shard):
             made = jnp.dot(hidden[...], down_full[shard], preferred_element_type=F32)
             for t in range(n_tp):
                 partials[t, shard] = made[:, t * local : (t + 1) * local].astype(BF16)
-            to_peers(step, lambda t: partials.at[t, shard], lambda t: arrived.at[t, shard])
-        for step in range(n_fs):
-            shard = lax.rem(fs - step + n_fs, n_fs)
-            from_peers(step, lambda t: arrived.at[t, shard])
-            conclude(shard, pl.ds(pl.multiple_of(shard * local, local), local))
+            for d in range(1, n_tp):
+                peer = other("tp", d)
+                remote(
+                    partials.at[peer, shard],
+                    arrived.at[tp, shard],
+                    part_send.at[shard, d - 1],
+                    part_recv.at[shard, d - 1],
+                    "tp",
+                    d,
+                ).start()
+
+        share(fs)
+        for step in range(n_fs - 1):
+            if step >= 1:
+                for sub in range(SUBS):
+                    serve(2, sub, step)
+            for way in range(2):
+                settle(2, step, (way,))
+                shard, valid = shard_sent(step + 1, way)
+                pl.when(valid)(functools.partial(share, shard))
+        for shard in range(n_fs):
+            from_peers(shard, lambda t: arrived.at[t, shard])
+            conclude(shard, slice(shard * local, (shard + 1) * local))
+            for d in range(1, n_tp):
+                mine = partials.at[other("tp", d), shard]
+                remote(
+                    mine, mine, part_send.at[shard, d - 1], part_recv.at[shard, d - 1], "tp", d
+                ).wait_send()
     else:
         for step in range(n_fs - 1):
             if step >= 1:
@@ -416,8 +460,11 @@
         for g in range(groups):
             conclude(g, slice(g * local, (g + 1) * local))
 
-    for copy in sent:
-        copy.wait_send()
+    for copy, valid in sent:
+        if valid is None:
+            copy.wait_send()
+        else:
+            pl.when(valid)(copy.wait_send)
 
 
 def shards(
@@ -470,10 +517,10 @@
             pltpu.VMEM((length, hidden_width), BF16),
             pltpu.VMEM((n_tp, groups, length, local), BF16),
             pltpu.VMEM((n_tp, groups, length, local), BF16),
-            dma((3, SUBS, hops)),
-            dma((3, SUBS, hops)),
-            dma((3, SUBS, hops, reps)),
-            dma((3, SUBS, hops, reps)),
+            dma((3, SUBS, 2 * hops)),
+            dma((3, SUBS, 2 * hops)),
+            dma((3, SUBS, 2 * hops, reps)),
+            dma((3, SUBS, 2 * hops, reps)),
             dma((hops,)),
             dma((hops,)),
             dma((hops, reps)),

time: 317 us -> 216 us (0.68)
  the two profiles are of different devices: /device:TPU:11 before, /device:TPU:0 now
where the time goes in v2:
time: 216 us; the launch traced here: 215 us
  Pallas kernels  199 us (92%)
  other arithmetic  10.1 us (5%)
  local copies, waits for them, and re-layouts  5.87 us (3%)
    pallas_call x1, Pallas kernels, shards(): pl.pallas_call(functools.partial(block_kernel, sizes), out_shape=jax.Shap...  199 us

profile of v2, /device:TPU:0, one launch (start us, length us, event | category | flops | bytes accessed | tf_op | source)
XLA Modules:
  0.0 214.5 jit_solution(10177358644888191833)
XLA Ops:
  0.0 1.3 pad_maximum_fusion.1.scale_pair
  1.3 1.3 pad_maximum_fusion.gains
  2.6 1.6 convert_element_type.12.pool_own
  4.2 0.0 copy-start
  4.2 2.3 %copy.16 = bf16[96,8,4,128]{3,1,2,0:T(8,128)(2,1)} copy(bf16[96,8,4,128]{3,2,1,0:T(4,128)(2,1)} %bitcast.10) | data formatting | bytes 1572864
  6.5 3.2 %convert_element_type.13.gate_own = bf16[512,1536]{1,0:T(8,128)(2,1)} convert(f32[512,1536]{1,0:T(8,128)} %param.18) | non-fusion elementwise | flops 786432 | bytes 4718592 | tf_op jit(solution)/shard_map/convert_element_type | solution.py:548
  9.7 0.0 copy-done
  9.7 0.0 copy-start.1
  9.7 1.3 convert_element_type.14.up_own
  11.1 1.1 copy-done.1
  12.2 1.3 convert_element_type.15.down_own
  13.5 198.5 %shard_map.127 = bf16[768,512]{1,0:T(8,128)(2,1)} custom-call(bf16[768,512]{1,0:T(8,128)(2,1)} %bitcast.9, f32[2,512]{1,0:T(2,128)} %pad_maximum_fusion.gains, f32[1,512]{1,0:T(1,128)} %bitcast.11, f32[1,512]{1,0:T(1,128)} %bitcast.12, f32[2,384]{1,0:T(2,128)} %pad_maximum_fusion.1.scale_pair, f32[3,1536]{1,0:T(4,128)} %gate_taps.1, f32[3,1536]{1,0:T(4,128)} %up_taps.1, ...), custom_call_target="tpu_custom_call" | custom-call | tf_op jit(solution)/shard_map/pallas_call | solution.py:498
  212.1 2.4 %reshape.15 = bf16[1,768,4,128]{3,2,1,0:T(4,128)(2,1)} reshape(bf16[768,512]{1,0:T(8,128)(2,1)} %shard_map.127) | data formatting | bytes 1572864 | tf_op jit(solution)/shard_map/reshape | solution.py:552
Async XLA Ops:
  4.2 5.5 %copy-start = (f32[512,1536]{1,0:T(8,128)S(1)}, f32[512,1536]{1,0:T(8,128)}, u32[]{:S(2)}) copy-start(f32[512,1536]{1,0:T(8,128)} %param.19) | copy-start | bytes 9437188
  9.7 2.5 %copy-start.1 = (f32[1536,512]{1,0:T(8,128)S(1)}, f32[1536,512]{1,0:T(8,128)}, u32[]{:S(2)}) copy-start(f32[1536,512]{1,0:T(8,128)} %param.24) | copy-start | bytes 9437188
